TPU v7x, 32 devices: a whole 2x2x4 slice. The times are simulated.
32 devices in a mesh: sp: 8 (over z, x), tp: 4 (over y, core).
Axes of the slice: x: 2, y: 2, z: 4, core: 2. Of those that a mesh axis runs over, the one named last changes fastest.
Arguments:
- queries: bfloat16 [2048, 1024], P('sp', 'tp'), may hold values from -6 to 6
- keys: bfloat16 [2048, 256], P('sp'), may hold values from -6 to 6
- values: bfloat16 [2048, 256], P('sp'), may hold values from -6 to 6
- sink: float32 [16], P('tp'), may hold values from 3 to 6
- w_out: bfloat16 [1024, 2048], P('tp'), may hold values from -0.1875 to 0.1875
- stream: bfloat16 [2048, 2048], P(('sp', 'tp')), may hold values from -6 to 6
- gain: bfloat16 [2048], replicated, may hold values from 0.099609375 to 1.8984375
- routes: int32 [2048, 4], P('sp'), may hold values from 0 to 63, all different within a row; in each aligned block of 64 rows (0 to 63, 64 to 127, ...) at most 8 rows name the same one
- route_weights: float32 [2048, 4], P('sp'), may hold values from 0.2 to 1
- w_gate: bfloat16 [64, 1024, 2048], P('sp', 'tp'), may hold values from -0.125 to 0.125
- w_up: bfloat16 [64, 1024, 2048], P('sp', 'tp'), may hold values from -0.125 to 0.125
- w_down: bfloat16 [64, 1024, 2048], P('sp', None, 'tp'), may hold values from -0.1875 to 0.1875
- shared_gate: bfloat16 [1024, 2048], P('tp'), may hold values from -0.125 to 0.125
- shared_up: bfloat16 [1024, 2048], P('tp'), may hold values from -0.125 to 0.125
- shared_down: bfloat16 [1024, 2048], P(None, 'tp'), may hold values from -0.1875 to 0.1875
Outputs:
- layer_out: bfloat16 [2048, 2048], P('sp', 'tp')
Inputs may be any that keep to these rules, and one draw needn't show every extreme that they name: `routes`: in each aligned block of 64 rows no expert is named in more than 8 rows, and some blocks reach 8; a row names 4 different experts.
All inputs are finite; a program needn't handle non-finite values.
Results may differ from a plain program's by a relative error of at most 0.014.
Values may be sent and summed in bfloat16 or wider, within the bound.
A program may use at most 128 MiB of HBM per device.

v0:
```python
import jax
import jax.numpy as jnp
from jax import lax
from jax.sharding import PartitionSpec as P

D = 2048
HEADS = 16
KV_HEADS = 4
HD = 64
WINDOW = 128
EXPERTS = 64
TOPK = 4
NORM_EPS = 1e-05


def with_halo(array, sides, width):
    for axis, dim in sides:
        devices, length = (lax.axis_size(axis), array.shape[dim])
        up = [(i, (i + 1) % devices) for i in range(devices - 1)]
        down = [(j, i) for i, j in up]
        last = lax.slice_in_dim(array, length - width, length, axis=dim)
        leading = lax.slice_in_dim(array, 0, width, axis=dim)
        before = lax.ppermute(last, axis, up)
        after = lax.ppermute(leading, axis, down)
        array = jnp.concatenate([before, array, after], axis=dim)
    return array


def slot_ids(block_routes, capacity):
    flat_routes = block_routes.reshape(-1)
    hit_table = (flat_routes[:, None] == jnp.arange(EXPERTS)[None, :]).astype(jnp.int32)
    earlier = jnp.cumsum(hit_table, axis=0) - hit_table
    slot_rank = jnp.sum(earlier * hit_table, axis=1)
    return flat_routes * capacity + slot_rank


def local(
    queries,
    keys,
    values,
    sink,
    w_out,
    stream,
    gain,
    routes,
    route_weights,
    w_gate,
    w_up,
    w_down,
    shared_gate,
    shared_up,
    shared_down,
):
    tok_dev = queries.shape[0]
    n_tp = lax.axis_size("tp")
    n_sp = lax.axis_size("sp")
    tp_idx = lax.axis_index("tp")
    sp_idx = lax.axis_index("sp")
    heads_dev = HEADS // n_tp
    group = HEADS // KV_HEADS
    kv_head = tp_idx * heads_dev // group
    key_own = lax.dynamic_slice_in_dim(keys, kv_head * HD, HD, 1)
    value_own = lax.dynamic_slice_in_dim(values, kv_head * HD, HD, 1)
    paired = jnp.concatenate([key_own, value_own], axis=1)
    padded = with_halo(paired, (("sp", 0),), WINDOW)
    blocks = tok_dev // WINDOW
    framed = padded.reshape(blocks + 2, WINDOW, 2 * HD)
    banded = jnp.concatenate([framed[:-2], framed[1:-1], framed[2:]], axis=1)
    key_band = banded[:, :, :HD]
    value_band = banded[:, :, HD:]
    query_blocks = queries.reshape(blocks, WINDOW, heads_dev, HD)
    scores = jnp.einsum(
        "nqhd,njd->nhqj", query_blocks, key_band, preferred_element_type=jnp.float32
    ) * HD ** (-0.5)
    offset = sp_idx * tok_dev
    seq_total = tok_dev * n_sp
    query_pos = (
        offset + jnp.arange(blocks)[:, None, None] * WINDOW + jnp.arange(WINDOW)[None, :, None]
    )
    key_pos = (
        offset
        - WINDOW
        + jnp.arange(blocks)[:, None, None] * WINDOW
        + jnp.arange(3 * WINDOW)[None, None, :]
    )
    allowed = (jnp.abs(query_pos - key_pos) <= WINDOW) & (key_pos >= 0) & (key_pos < seq_total)
    scores = jnp.where(allowed[:, None], scores, -jnp.inf)
    sink_level = sink.reshape(1, heads_dev, 1, 1)
    row_peak = jnp.maximum(scores.max(-1, keepdims=True), sink_level)
    probabilities = jnp.exp(scores - row_peak)
    denominator = probabilities.sum(-1, keepdims=True) + jnp.exp(sink_level - row_peak)
    weights = (probabilities / denominator).astype(jnp.bfloat16)
    attended = jnp.einsum("nhqj,njd->nqhd", weights, value_band, preferred_element_type=jnp.float32)
    attended = attended.astype(jnp.bfloat16).reshape(tok_dev, heads_dev * HD)
    rows_dev = tok_dev // n_tp
    d_dev = w_down.shape[2]
    projected = lax.psum_scatter(
        jnp.dot(attended, w_out, preferred_element_type=jnp.float32),
        "tp",
        scatter_dimension=0,
        tiled=True,
    )
    mixed_rows = (stream.astype(jnp.float32) + projected).astype(jnp.bfloat16)
    whole_rows = lax.all_gather(mixed_rows, "tp", axis=0, tiled=True)
    wide_rows = whole_rows.astype(jnp.float32)
    scale_rows = lax.rsqrt(jnp.mean(wide_rows * wide_rows, axis=-1, keepdims=True) + NORM_EPS)
    normed = (wide_rows * scale_rows * gain.astype(jnp.float32)).astype(jnp.bfloat16)
    residual = lax.dynamic_slice_in_dim(wide_rows, tp_idx * d_dev, d_dev, 1)
    exp_dev = w_gate.shape[0]
    capacity = max(1, 2 * tok_dev * TOPK // (n_tp * EXPERTS))
    slot_count = EXPERTS * capacity
    blocked_routes = routes.reshape(n_tp, rows_dev, TOPK)
    destination = jax.vmap(lambda block_routes: slot_ids(block_routes, capacity))(blocked_routes)
    slot_select = destination[:, None, :] == jnp.arange(slot_count)[None, :, None]
    slot_select = slot_select.reshape(n_tp, slot_count, rows_dev, TOPK).astype(jnp.float32)
    dispatch_table = jnp.sum(slot_select, axis=-1).astype(jnp.bfloat16)
    combine_table = jnp.sum(slot_select * route_weights.reshape(n_tp, 1, rows_dev, TOPK), axis=-1)
    normed_blocks = normed.reshape(n_tp, rows_dev, D)
    own_table = lax.dynamic_index_in_dim(dispatch_table, tp_idx, 0, keepdims=False)
    own_rows = lax.dynamic_index_in_dim(normed_blocks, tp_idx, 0, keepdims=False)
    outgoing = jnp.dot(own_table, own_rows, preferred_element_type=jnp.float32).astype(jnp.bfloat16)
    arrived = lax.all_to_all(outgoing, "sp", split_axis=0, concat_axis=0, tiled=True)
    arrived = arrived.reshape(1, n_sp, exp_dev, capacity, D)
    piece_rows = lax.all_gather(arrived, "tp", axis=0, tiled=True)
    gate_act = jnp.einsum(
        "tsecd,efd->tsecf", piece_rows, w_gate, preferred_element_type=jnp.float32
    )
    up_act = jnp.einsum("tsecd,efd->tsecf", piece_rows, w_up, preferred_element_type=jnp.float32)
    hidden = (jax.nn.silu(gate_act) * up_act).astype(jnp.bfloat16)
    shared_gate_act = jnp.einsum(
        "td,fd->tf", normed, shared_gate, preferred_element_type=jnp.float32
    )
    shared_up_act = jnp.einsum("td,fd->tf", normed, shared_up, preferred_element_type=jnp.float32)
    shared_hidden = (jax.nn.silu(shared_gate_act) * shared_up_act).astype(jnp.bfloat16)
    shared_hidden = shared_hidden.reshape(1, 1, 1, tok_dev, shared_hidden.shape[1])
    expert_piece = lax.all_gather(hidden, "tp", axis=4, tiled=True)
    shared_piece = lax.all_gather(shared_hidden, "tp", axis=4, tiled=True)
    piece_width = expert_piece.shape[4]
    routed_total = jnp.einsum(
        "tsecf,efd->tsecd", expert_piece, w_down, preferred_element_type=jnp.float32
    )
    shared_total = jnp.dot(
        shared_piece.reshape(tok_dev, piece_width), shared_down, preferred_element_type=jnp.float32
    )
    returned = lax.all_to_all(
        routed_total.astype(jnp.bfloat16), "sp", split_axis=1, concat_axis=1, tiled=True
    )
    returned = returned.reshape(n_tp, slot_count, d_dev).astype(jnp.float32)
    routed = jnp.einsum("tmr,tmd->trd", combine_table, returned, precision=lax.Precision.HIGHEST)
    routed = routed.reshape(tok_dev, d_dev)
    return (residual + routed + shared_total).astype(jnp.bfloat16)


def solution(mesh):
    placed = (
        P("sp", "tp"),
        P("sp", None),
        P("sp", None),
        P("tp"),
        P("tp", None),
        P(("sp", "tp"), None),
        P(),
        P("sp", None),
        P("sp", None),
        P("sp", "tp", None),
        P("sp", "tp", None),
        P("sp", None, "tp"),
        P("tp", None),
        P("tp", None),
        P(None, "tp"),
    )
    return jax.shard_map(
        local, mesh=mesh, in_specs=placed, out_specs=P("sp", "tp"), check_vma=False
    )
```

profile of v0, /device:TPU:0, one launch (start us, length us, event | category | flops | bytes accessed | tf_op | source)
XLA Modules:
  0.0 317.8 jit_solution(6857469026317906916)
XLA Ops:
  7.7 4.9 %collective-permute-start = (bf16[128,128]{1,0:T(8,128)(2,1)S(1)}, bf16[128,128]{1,0:T(8,128)(2,1)S(1)}, u32[]{:S(2)}, u32[]{:S(2)}) collective-permute-start(bf16[128,128]{1,0:T(8,128)(2,1)S(1)} %get-tuple-element.10), channel_id=1, source_target_pairs={{0,4},{4,8},{8,12},{12,16},{16,20},{20,24},{24,28},{1,5},{5,9},{9,... | collective-permute-start | bytes 98312 | tf_op jit(solution)/shard_map/ppermute | solution.py:23
  12.6 1.3 collective-permute-start.1
  15.7 2.7 collective-permute-done.1
  20.4 1.8 fusion.27
  22.3 32.5 %reduce-scatter.2.cloned.1.call-done = f32[64,2048]{1,0:T(8,128)} async-done(((f32[256,2048]{1,0:T(8,128)}), f32[64,2048]{1,0:T(8,128)}) %reduce-scatter.2.cloned.1.call-update) | async-done | bytes 524304 | tf_op jit(solution)/shard_map/reduce_scatter | solution.py:97
  54.7 1.8 add_convert_fusion
  57.2 2.4 reduce-window.6
  60.4 1.3 convert_reduce_fusion
  61.7 11.7 %all-gather.5.cloned.1.call-done = bf16[256,2048]{1,0:T(8,128)(2,1)} async-done(((bf16[64,2048]{1,0:T(8,128)(2,1)}), bf16[256,2048]{1,0:T(8,128)(2,1)}) %all-gather.5.cloned.1.call-update) | async-done | bytes 1048592 | tf_op jit(solution)/shard_map/all_gather | solution.py:104
  73.4 1.5 multiply_reduce_fusion
  74.9 1.5 multiply_convert_fusion
  77.2 53.9 %all_to_all.14 = bf16[8,64,2048]{2,1,0:T(8,128)(2,1)S(1)} all-to-all(bf16[8,64,2048]{2,1,0:T(8,128)(2,1)S(1)} %bitcast.114), channel_id=1, replica_groups=mesh['sp'=8,'tp'=4] {'sp'}, dimensions={0} | all-to-all | bytes 4194304 | tf_op jit(solution)/shard_map/all_to_all | solution.py:122
  131.1 1.5 copy.68
  132.8 56.3 %all-gather.7.cloned.1.call-done = bf16[4,8,8,8,2048]{4,3,1,0,2:T(8,128)(2,1)} async-done(((bf16[1,8,8,8,2048]{4,3,1,0,2:T(8,128)(2,1)}), bf16[4,8,8,8,2048]{4,3,1,0,2:T(8,128)(2,1)}) %all-gather.7.cloned.1.call-update) | async-done | bytes 8388624 | tf_op jit(solution)/shard_map/all_gather | solution.py:124
  189.2 8.1 %fusion.4 = f32[8,4,8,8,256]{4,3,2,1,0:T(8,128)S(1)} fusion(bf16[4,8,8,8,2048]{4,3,1,0,2:T(8,128)(2,1)} %all-gather.7.cloned.1.call-done, bf16[8,256,2048]{2,1,0:T(8,128)(2,1)} %param.24), kind=kOutput, calls=%fused_computation.4 | convolution fusion | flops 2147483648 | bytes 18874368 | tf_op jit(solution)/shard_map/tsecd,efd->tsecf/dot_general | solution.py:125
  197.3 11.4 %fusion.6 = bf16[4,8,8,8,256]{4,3,1,0,2:T(8,128)(2,1)} fusion(f32[8,4,8,8,256]{4,3,2,1,0:T(8,128)S(1)} %fusion.4, bf16[4,8,8,8,2048]{4,3,1,0,2:T(8,128)(2,1)} %all-gather.7.cloned.1.call-done, bf16[8,256,2048]{2,1,0:T(8,128)(2,1)} %param.25), kind=kOutput, calls=%fused_computation.8 | convolution fusion | flops 2150629376 | bytes 19922944 | tf_op jit(solution)/shard_map/tsecd,efd->tsecf/dot_general | solution.py:128
  208.7 35.2 %all-gather.9.cloned.1.call-done = bf16[4,8,8,8,1024]{4,3,1,0,2:T(8,128)(2,1)} async-done(((bf16[4,8,8,8,256]{4,3,1,0,2:T(8,128)(2,1)}), bf16[4,8,8,8,1024]{4,3,1,0,2:T(8,128)(2,1)}) %all-gather.9.cloned.1.call-update) | async-done | bytes 4194320 | tf_op jit(solution)/shard_map/all_gather | solution.py:136
  243.8 7.0 %convert_bitcast_fusion = bf16[4,8,8,8,512]{4,3,1,0,2:T(8,128)(2,1)S(1)} fusion(bf16[4,8,8,8,1024]{4,3,1,0,2:T(8,128)(2,1)} %all-gather.9.cloned.1.call-done, bf16[8,1024,512]{2,1,0:T(8,128)(2,1)} %param.26), kind=kOutput, calls=%fused_computation.14 | convolution fusion | flops 2148532224 | bytes 14680064 | tf_op jit(solution)/shard_map/tsecf,efd->tsecd/dot_general | solution.py:139
  250.8 1.6 copy.69
  252.4 5.6 %all-to-all-start.1 = ((bf16[4,8,8,8,512]{4,3,0,2,1:T(8,128)(2,1)}), bf16[4,8,8,8,512]{4,3,0,2,1:T(8,128)(2,1)S(1)}, u32[]{:S(2)}, u32[]{:S(2)}) async-start(bf16[4,8,8,8,512]{4,3,0,2,1:T(8,128)(2,1)} %copy.69), calls=%async_computation.2 | async-start | bytes 4194304 | tf_op jit(solution)/shard_map/all_to_all | solution.py:145
  258.1 1.6 convert_element_type.61
  261.3 7.4 %all-gather = bf16[256,1024]{1,0:T(8,128)(2,1)} all-gather(bf16[256,256]{1,0:T(8,128)(2,1)S(1)} %fusion.16), channel_id=2, replica_groups=mesh['sp'=8,'tp'=4] {'tp'}, dimensions={1}, use_global_device_ids=true | all-gather | bytes 655360 | tf_op jit(solution)/shard_map/all_gather | solution.py:137
  268.7 38.0 %all-to-all-done.1 = bf16[4,8,8,8,512]{4,3,0,2,1:T(8,128)(2,1)S(1)} async-done(((bf16[4,8,8,8,512]{4,3,0,2,1:T(8,128)(2,1)}), bf16[4,8,8,8,512]{4,3,0,2,1:T(8,128)(2,1)S(1)}, u32[]{:S(2)}, u32[]{:S(2)}) %all-to-all-start.1) | async-done | bytes 2097184 | tf_op jit(solution)/shard_map/all_to_all | solution.py:145
  307.8 1.2 fusion.42
  (84 shorter events, 12.3 us)
Async XLA Ops:
  6.5 13.8 %copy-start = (bf16[256,2048]{1,0:T(8,128)(2,1)S(1)}, bf16[256,2048]{1,0:T(8,128)(2,1)}, u32[]{:S(2)}) copy-start(bf16[256,2048]{1,0:T(8,128)(2,1)} %param.19) | copy-start | bytes 3145732
  6.5 48.2 %reduce-scatter.2.cloned.1.call-start = ((), (), s32[]{:S(2)}) async-start(), calls=%async_computation.3 | async-start | bytes 2621440 | tf_op jit(solution)/shard_map/reduce_scatter | solution.py:97
  6.5 12.9 %copy-start.13 = (f32[4]{0:T(128)S(1)}, f32[4]{0:T(128)}, u32[]{:S(2)}) copy-start(f32[4]{0:T(128)} %param.18) | copy-start | bytes 52
  7.7 8.0 %collective-permute-start = (bf16[128,128]{1,0:T(8,128)(2,1)S(1)}, bf16[128,128]{1,0:T(8,128)(2,1)S(1)}, u32[]{:S(2)}, u32[]{:S(2)}) collective-permute-start(bf16[128,128]{1,0:T(8,128)(2,1)S(1)} %get-tuple-element.10), channel_id=1, source_target_pairs={{0,4},{4,8},{8,12},{12,16},{16,20},{20,24},{24,28},{1,5},{5,9},{9,... | collective-permute-start | bytes 98312 | tf_op jit(solution)/shard_map/ppermute | solution.py:23
  12.6 5.8 %collective-permute-start.1 = (bf16[128,128]{1,0:T(8,128)(2,1)S(1)}, bf16[128,128]{1,0:T(8,128)(2,1)S(1)}, u32[]{:S(2)}, u32[]{:S(2)}) collective-permute-start(bf16[128,128]{1,0:T(8,128)(2,1)S(1)} %get-tuple-element.11), channel_id=1, source_target_pairs={{4,0},{8,4},{12,8},{16,12},{20,16},{24,20},{28,24},{5,1},{9,5},{13... | collective-permute-start | bytes 98312 | tf_op jit(solution)/shard_map/ppermute | solution.py:24
  20.4 34.4 %copy-start.9 = (bf16[64,2048]{1,0:T(8,128)(2,1)S(1)}, bf16[64,2048]{1,0:T(8,128)(2,1)}, u32[]{:S(2)}) copy-start(bf16[64,2048]{1,0:T(8,128)(2,1)} %param.20) | copy-start | bytes 786436
  22.2 34.4 %copy-start.10 = (s32[256,4]{0,1:T(4,128)S(1)}, s32[256,4]{0,1:T(4,128)}, u32[]{:S(2)}) copy-start(s32[256,4]{0,1:T(4,128)} %param.22) | copy-start | bytes 12292
  22.2 38.1 %copy-start.11 = (f32[256,4]{0,1:T(4,128)S(1)}, f32[256,4]{0,1:T(4,128)}, u32[]{:S(2)}) copy-start(f32[256,4]{0,1:T(4,128)} %param.23) | copy-start | bytes 12292
  22.2 38.2 %copy-start.12 = (bf16[2048]{0:T(1024)(128)(2,1)S(1)}, bf16[2048]{0:T(1024)(128)(2,1)}, u32[]{:S(2)}) copy-start(bf16[2048]{0:T(1024)(128)(2,1)} %param.21) | copy-start | bytes 12292
  22.2 51.2 %all-gather.5.cloned.1.call-start = ((), (), s32[]{:S(2)}) async-start(), calls=%async_computation.4 | async-start | bytes 1310720 | tf_op jit(solution)/shard_map/all_gather | solution.py:104
  56.5 132.6 %all-gather.7.cloned.1.call-start = ((), (), s32[]{:S(2)}) async-start(), calls=%async_computation.5 | async-start | bytes 10485760 | tf_op jit(solution)/shard_map/all_gather | solution.py:124
  76.5 54.6 %copy-start.3 = (bf16[256,2048]{1,0:T(8,128)(2,1)}, bf16[256,2048]{1,0:T(8,128)(2,1)S(1)}, u32[]{:S(2)}) copy-start(bf16[256,2048]{1,0:T(8,128)(2,1)S(1)} %multiply_convert_fusion) | copy-start | bytes 3145732
  132.6 111.2 %all-gather.9.cloned.1.call-start = ((), (), s32[]{:S(2)}) async-start(), calls=%async_computation.6 | async-start | bytes 5242880 | tf_op jit(solution)/shard_map/all_gather | solution.py:136
  252.4 5.6 %copy-start.2 = (bf16[256,2048]{1,0:T(8,128)(2,1)S(1)}, bf16[256,2048]{1,0:T(8,128)(2,1)}, u32[]{:S(2)}) copy-start(bf16[256,2048]{1,0:T(8,128)(2,1)} %all-gather.5.cloned.1.call-done) | copy-start | bytes 3145732
  252.4 54.3 %all-to-all-start.1 = ((bf16[4,8,8,8,512]{4,3,0,2,1:T(8,128)(2,1)}), bf16[4,8,8,8,512]{4,3,0,2,1:T(8,128)(2,1)S(1)}, u32[]{:S(2)}, u32[]{:S(2)}) async-start(bf16[4,8,8,8,512]{4,3,0,2,1:T(8,128)(2,1)} %copy.69), calls=%async_computation.2 | async-start | bytes 4194304 | tf_op jit(solution)/shard_map/all_to_all | solution.py:145
  258.1 1.6 copy-start.4
  258.1 2.3 copy-start.7
  258.1 2.8 copy-start.14
  306.7 1.0 copy-start.6
  307.8 2.3 copy-start.5
  307.8 2.3 copy-start.8
  307.8 3.5 %copy-start.1 = (bf16[256,2048]{1,0:T(8,128)(2,1)S(1)}, bf16[256,2048]{1,0:T(8,128)(2,1)}, u32[]{:S(2)}) copy-start(bf16[256,2048]{1,0:T(8,128)(2,1)} %param.19) | copy-start | bytes 3145732
Sparse Core Ops, SparseCore 0:
  22.3 32.3 reduce-scatter.1
  56.7 16.6 all-gather.4
  132.7 56.3 all-gather.6
  208.8 34.9 all-gather.8
where the time goes:
time: 318 us
  waiting for transfers between devices  176 us (55%)
  blocking collectives  61.2 us (19%)
  matrix products  33.1 us (10%)
  between operations  13.5 us (4%)
  other arithmetic  12.7 us (4%)
  starting transfers between devices  12.1 us (4%)
  local copies, waits for them, and re-layouts  8.65 us (3%)
    all_gather x1, waiting for transfers between devices, local(): piece_rows = lax.all_gather(arrived, 'tp', axis=0, tiled=True)  56.3 us
    all_to_all x1, blocking collectives, local(): lax.all_to_all(outgoing, 'sp', split_axis=0, concat_axis=0, tiled=True)  53.9 us
    all_to_all x1, waiting for transfers between devices, local(): lax.all_to_all(routed_total.astype(jnp.bfloat16), 'sp', split_axis=1, con...  38 us
    all_gather x1, waiting for transfers between devices, local(): expert_piece = lax.all_gather(hidden, 'tp', axis=4, tiled=True)  35.2 us
    reduce_scatter x1, waiting for transfers between devices, local(): lax.psum_scatter(jnp.dot(attended, w_out, preferred_element_type=jnp.floa...  32.5 us
    all_gather x1, waiting for transfers between devices, local(): whole_rows = lax.all_gather(mixed_rows, 'tp', axis=0, tiled=True)  11.7 us
    dot_general x1, matrix products, local(): jnp.einsum('tsecd,efd->tsecf', piece_rows, w_up, preferred_element_type=j...  11.4 us
    dot_general x1, matrix products, local(): jnp.einsum('tsecd,efd->tsecf', piece_rows, w_gate, preferred_element_type...  8.13 us
  transfers between devices with their start and end apart: 7, of which 6 were waited for; matrix products, arithmetic and copies ran while one was open for 3% of the time, Pallas kernels for 0%

commit v1 on v0

--- a/solution.py
+++ b/solution.py
@@ -142,8 +142,14 @@
     shared_total = jnp.dot(
         shared_piece.reshape(tok_dev, piece_width), shared_down, preferred_element_type=jnp.float32
     )
-    returned = lax.all_to_all(
-        routed_total.astype(jnp.bfloat16), "sp", split_axis=1, concat_axis=1, tiled=True
+    returned = jnp.concatenate(
+        lax.all_to_all(
+            jnp.stack(jnp.split(routed_total.astype(jnp.bfloat16), lax.axis_size("sp"), axis=1)),
+            "sp",
+            0,
+            0,
+        ),
+        axis=1,
     )
     returned = returned.reshape(n_tp, slot_count, d_dev).astype(jnp.float32)
     routed = jnp.einsum("tmr,tmd->trd", combine_table, returned, precision=lax.Precision.HIGHEST)

time: 318 us -> 322 us (1.013)
  local copies, waits for them, and re-layouts: 8.65 us -> 12.8 us
    unnamed x31 -> x38, local copies, waits for them, and re-layouts: 1.66 us -> 6.71 us
where the time goes in v1:
time: 322 us
  waiting for transfers between devices  176 us (55%)
  blocking collectives  61.2 us (19%)
  matrix products  33.1 us (10%)
  between operations  13.5 us (4%)
  local copies, waits for them, and re-layouts  12.8 us (4%)
  other arithmetic  12.7 us (4%)
  starting transfers between devices  12.1 us (4%)
    all_gather x1, waiting for transfers between devices, local(): piece_rows = lax.all_gather(arrived, 'tp', axis=0, tiled=True)  56.3 us
    all_to_all x1, blocking collectives, local(): lax.all_to_all(outgoing, 'sp', split_axis=0, concat_axis=0, tiled=True)  53.9 us
    all_to_all x1, waiting for transfers between devices, local(): lax.all_to_all(jnp.stack(jnp.split(routed_total.astype(jnp.bfloat16), lax...  38 us
    all_gather x1, waiting for transfers between devices, local(): expert_piece = lax.all_gather(hidden, 'tp', axis=4, tiled=True)  35.2 us
    reduce_scatter x1, waiting for transfers between devices, local(): lax.psum_scatter(jnp.dot(attended, w_out, preferred_element_type=jnp.floa...  32.5 us
    all_gather x1, waiting for transfers between devices, local(): whole_rows = lax.all_gather(mixed_rows, 'tp', axis=0, tiled=True)  11.7 us
    dot_general x1, matrix products, local(): jnp.einsum('tsecd,efd->tsecf', piece_rows, w_up, preferred_element_type=j...  11.4 us
    dot_general x1, matrix products, local(): jnp.einsum('tsecd,efd->tsecf', piece_rows, w_gate, preferred_element_type...  8.13 us
  transfers between devices with their start and end apart: 7, of which 6 were waited for; matrix products, arithmetic and copies ran while one was open for 3% of the time, Pallas kernels for 0%

profile of v1, /device:TPU:0, one launch (start us, length us, event | category | flops | bytes accessed | tf_op | source)
XLA Modules:
  0.0 322.0 jit_solution(17035566820541005674)
XLA Ops:
  7.7 4.9 %collective-permute-start = (bf16[128,128]{1,0:T(8,128)(2,1)S(1)}, bf16[128,128]{1,0:T(8,128)(2,1)S(1)}, u32[]{:S(2)}, u32[]{:S(2)}) collective-permute-start(bf16[128,128]{1,0:T(8,128)(2,1)S(1)} %get-tuple-element.10), channel_id=1, source_target_pairs={{0,4},{4,8},{8,12},{12,16},{16,20},{20,24},{24,28},{1,5},{5,9},{9,... | collective-permute-start | bytes 98312 | tf_op jit(solution)/shard_map/ppermute | solution.py:23
  12.6 1.3 collective-permute-start.1
  15.7 2.7 collective-permute-done.1
  20.4 1.8 fusion.35
  22.3 32.5 %reduce-scatter.2.cloned.1.call-done = f32[64,2048]{1,0:T(8,128)} async-done(((f32[256,2048]{1,0:T(8,128)}), f32[64,2048]{1,0:T(8,128)}) %reduce-scatter.2.cloned.1.call-update) | async-done | bytes 524304 | tf_op jit(solution)/shard_map/reduce_scatter | solution.py:97
  54.7 1.8 add_convert_fusion
  57.2 2.4 reduce-window.6
  60.4 1.3 convert_reduce_fusion
  61.7 11.7 %all-gather.5.cloned.1.call-done = bf16[256,2048]{1,0:T(8,128)(2,1)} async-done(((bf16[64,2048]{1,0:T(8,128)(2,1)}), bf16[256,2048]{1,0:T(8,128)(2,1)}) %all-gather.5.cloned.1.call-update) | async-done | bytes 1048592 | tf_op jit(solution)/shard_map/all_gather | solution.py:104
  73.4 1.5 multiply_reduce_fusion
  74.9 1.5 multiply_convert_fusion
  77.2 53.9 %all_to_all.14 = bf16[8,64,2048]{2,1,0:T(8,128)(2,1)S(1)} all-to-all(bf16[8,64,2048]{2,1,0:T(8,128)(2,1)S(1)} %bitcast.162), channel_id=1, replica_groups=mesh['sp'=8,'tp'=4] {'sp'}, dimensions={0} | all-to-all | bytes 4194304 | tf_op jit(solution)/shard_map/all_to_all | solution.py:122
  131.1 1.5 copy.65
  132.8 56.3 %all-gather.7.cloned.1.call-done = bf16[4,8,8,8,2048]{4,3,1,0,2:T(8,128)(2,1)} async-done(((bf16[1,8,8,8,2048]{4,3,1,0,2:T(8,128)(2,1)}), bf16[4,8,8,8,2048]{4,3,1,0,2:T(8,128)(2,1)}) %all-gather.7.cloned.1.call-update) | async-done | bytes 8388624 | tf_op jit(solution)/shard_map/all_gather | solution.py:124
  189.2 8.1 %fusion.4 = f32[8,4,8,8,256]{4,3,2,1,0:T(8,128)S(1)} fusion(bf16[4,8,8,8,2048]{4,3,1,0,2:T(8,128)(2,1)} %all-gather.7.cloned.1.call-done, bf16[8,256,2048]{2,1,0:T(8,128)(2,1)} %param.24), kind=kOutput, calls=%fused_computation.4 | convolution fusion | flops 2147483648 | bytes 18874368 | tf_op jit(solution)/shard_map/tsecd,efd->tsecf/dot_general | solution.py:125
  197.3 11.4 %fusion.6 = bf16[4,8,8,8,256]{4,3,1,0,2:T(8,128)(2,1)} fusion(f32[8,4,8,8,256]{4,3,2,1,0:T(8,128)S(1)} %fusion.4, bf16[4,8,8,8,2048]{4,3,1,0,2:T(8,128)(2,1)} %all-gather.7.cloned.1.call-done, bf16[8,256,2048]{2,1,0:T(8,128)(2,1)} %param.25), kind=kOutput, calls=%fused_computation.8 | convolution fusion | flops 2150629376 | bytes 19922944 | tf_op jit(solution)/shard_map/tsecd,efd->tsecf/dot_general | solution.py:128
  208.7 35.2 %all-gather.9.cloned.1.call-done = bf16[4,8,8,8,1024]{4,3,1,0,2:T(8,128)(2,1)} async-done(((bf16[4,8,8,8,256]{4,3,1,0,2:T(8,128)(2,1)}), bf16[4,8,8,8,1024]{4,3,1,0,2:T(8,128)(2,1)}) %all-gather.9.cloned.1.call-update) | async-done | bytes 4194320 | tf_op jit(solution)/shard_map/all_gather | solution.py:136
  243.8 7.0 %convert_bitcast_fusion = bf16[4,8,8,8,512]{4,3,1,0,2:T(8,128)(2,1)S(1)} fusion(bf16[4,8,8,8,1024]{4,3,1,0,2:T(8,128)(2,1)} %all-gather.9.cloned.1.call-done, bf16[8,1024,512]{2,1,0:T(8,128)(2,1)} %param.26), kind=kOutput, calls=%fused_computation.14 | convolution fusion | flops 2148532224 | bytes 14680064 | tf_op jit(solution)/shard_map/tsecf,efd->tsecd/dot_general | solution.py:139
  256.6 5.6 %all-to-all-start.1 = ((bf16[8,4,1,8,8,512]{5,4,1,3,2,0:T(8,128)(2,1)}), bf16[8,4,1,8,8,512]{5,4,1,3,2,0:T(8,128)(2,1)S(1)}, u32[]{:S(2)}, u32[]{:S(2)}) async-start(bf16[8,4,1,8,8,512]{5,4,1,3,2,0:T(8,128)(2,1)} %fusion.23), calls=%async_computation.2 | async-start | bytes 4194304 | tf_op jit(solution)/shard_map/all_to_all | solution.py:146
  262.3 1.6 convert_element_type.61
  265.5 7.4 %all-gather = bf16[256,1024]{1,0:T(8,128)(2,1)} all-gather(bf16[256,256]{1,0:T(8,128)(2,1)S(1)} %fusion.16), channel_id=2, replica_groups=mesh['sp'=8,'tp'=4] {'tp'}, dimensions={1}, use_global_device_ids=true | all-gather | bytes 655360 | tf_op jit(solution)/shard_map/all_gather | solution.py:137
  272.9 38.0 %all-to-all-done.1 = bf16[8,4,1,8,8,512]{5,4,1,3,2,0:T(8,128)(2,1)S(1)} async-done(((bf16[8,4,1,8,8,512]{5,4,1,3,2,0:T(8,128)(2,1)}), bf16[8,4,1,8,8,512]{5,4,1,3,2,0:T(8,128)(2,1)S(1)}, u32[]{:S(2)}, u32[]{:S(2)}) %all-to-all-start.1) | async-done | bytes 2097184 | tf_op jit(solution)/shard_map/all_to_all | solution.py:146
  311.9 1.2 fusion.50
  314.3 1.1 fusion.15
  (91 shorter events, 16.9 us)
Async XLA Ops:
  6.5 13.8 %copy-start = (bf16[256,2048]{1,0:T(8,128)(2,1)S(1)}, bf16[256,2048]{1,0:T(8,128)(2,1)}, u32[]{:S(2)}) copy-start(bf16[256,2048]{1,0:T(8,128)(2,1)} %param.19) | copy-start | bytes 3145732
  6.5 48.2 %reduce-scatter.2.cloned.1.call-start = ((), (), s32[]{:S(2)}) async-start(), calls=%async_computation.3 | async-start | bytes 2621440 | tf_op jit(solution)/shard_map/reduce_scatter | solution.py:97
  6.5 12.9 %copy-start.13 = (f32[4]{0:T(128)S(1)}, f32[4]{0:T(128)}, u32[]{:S(2)}) copy-start(f32[4]{0:T(128)} %param.18) | copy-start | bytes 52
  7.7 8.0 %collective-permute-start = (bf16[128,128]{1,0:T(8,128)(2,1)S(1)}, bf16[128,128]{1,0:T(8,128)(2,1)S(1)}, u32[]{:S(2)}, u32[]{:S(2)}) collective-permute-start(bf16[128,128]{1,0:T(8,128)(2,1)S(1)} %get-tuple-element.10), channel_id=1, source_target_pairs={{0,4},{4,8},{8,12},{12,16},{16,20},{20,24},{24,28},{1,5},{5,9},{9,... | collective-permute-start | bytes 98312 | tf_op jit(solution)/shard_map/ppermute | solution.py:23
  12.6 5.8 %collective-permute-start.1 = (bf16[128,128]{1,0:T(8,128)(2,1)S(1)}, bf16[128,128]{1,0:T(8,128)(2,1)S(1)}, u32[]{:S(2)}, u32[]{:S(2)}) collective-permute-start(bf16[128,128]{1,0:T(8,128)(2,1)S(1)} %get-tuple-element.11), channel_id=1, source_target_pairs={{4,0},{8,4},{12,8},{16,12},{20,16},{24,20},{28,24},{5,1},{9,5},{13... | collective-permute-start | bytes 98312 | tf_op jit(solution)/shard_map/ppermute | solution.py:24
  20.4 34.4 %copy-start.9 = (bf16[64,2048]{1,0:T(8,128)(2,1)S(1)}, bf16[64,2048]{1,0:T(8,128)(2,1)}, u32[]{:S(2)}) copy-start(bf16[64,2048]{1,0:T(8,128)(2,1)} %param.20) | copy-start | bytes 786436
  22.2 34.4 %copy-start.10 = (s32[256,4]{0,1:T(4,128)S(1)}, s32[256,4]{0,1:T(4,128)}, u32[]{:S(2)}) copy-start(s32[256,4]{0,1:T(4,128)} %param.22) | copy-start | bytes 12292
  22.2 38.1 %copy-start.11 = (f32[256,4]{0,1:T(4,128)S(1)}, f32[256,4]{0,1:T(4,128)}, u32[]{:S(2)}) copy-start(f32[256,4]{0,1:T(4,128)} %param.23) | copy-start | bytes 12292
  22.2 38.2 %copy-start.12 = (bf16[2048]{0:T(1024)(128)(2,1)S(1)}, bf16[2048]{0:T(1024)(128)(2,1)}, u32[]{:S(2)}) copy-start(bf16[2048]{0:T(1024)(128)(2,1)} %param.21) | copy-start | bytes 12292
  22.2 51.2 %all-gather.5.cloned.1.call-start = ((), (), s32[]{:S(2)}) async-start(), calls=%async_computation.4 | async-start | bytes 1310720 | tf_op jit(solution)/shard_map/all_gather | solution.py:104
  56.5 132.6 %all-gather.7.cloned.1.call-start = ((), (), s32[]{:S(2)}) async-start(), calls=%async_computation.5 | async-start | bytes 10485760 | tf_op jit(solution)/shard_map/all_gather | solution.py:124
  76.5 54.6 %copy-start.3 = (bf16[256,2048]{1,0:T(8,128)(2,1)}, bf16[256,2048]{1,0:T(8,128)(2,1)S(1)}, u32[]{:S(2)}) copy-start(bf16[256,2048]{1,0:T(8,128)(2,1)S(1)} %multiply_convert_fusion) | copy-start | bytes 3145732
  132.6 111.2 %all-gather.9.cloned.1.call-start = ((), (), s32[]{:S(2)}) async-start(), calls=%async_computation.6 | async-start | bytes 5242880 | tf_op jit(solution)/shard_map/all_gather | solution.py:136
  256.6 5.6 %copy-start.2 = (bf16[256,2048]{1,0:T(8,128)(2,1)S(1)}, bf16[256,2048]{1,0:T(8,128)(2,1)}, u32[]{:S(2)}) copy-start(bf16[256,2048]{1,0:T(8,128)(2,1)} %all-gather.5.cloned.1.call-done) | copy-start | bytes 3145732
  256.6 54.3 %all-to-all-start.1 = ((bf16[8,4,1,8,8,512]{5,4,1,3,2,0:T(8,128)(2,1)}), bf16[8,4,1,8,8,512]{5,4,1,3,2,0:T(8,128)(2,1)S(1)}, u32[]{:S(2)}, u32[]{:S(2)}) async-start(bf16[8,4,1,8,8,512]{5,4,1,3,2,0:T(8,128)(2,1)} %fusion.23), calls=%async_computation.2 | async-start | bytes 4194304 | tf_op jit(solution)/shard_map/all_to_all | solution.py:146
  262.3 1.6 copy-start.4
  262.3 2.3 copy-start.7
  262.3 2.8 copy-start.14
  310.9 1.0 copy-start.6
  311.9 2.3 copy-start.5
  311.9 2.3 copy-start.8
  311.9 3.5 %copy-start.1 = (bf16[256,2048]{1,0:T(8,128)(2,1)S(1)}, bf16[256,2048]{1,0:T(8,128)(2,1)}, u32[]{:S(2)}) copy-start(bf16[256,2048]{1,0:T(8,128)(2,1)} %param.19) | copy-start | bytes 3145732
Sparse Core Ops, SparseCore 0:
  22.3 32.3 reduce-scatter.1
  56.7 16.6 all-gather.4
  132.7 56.3 all-gather.6
  208.8 34.9 all-gather.8
